TPU v7x, 32 devices: a whole 2x2x4 slice. The times are simulated.
32 devices in a mesh: sp: 8 (over z, x), tp: 4 (over y, core).
Axes of the slice: x: 2, y: 2, z: 4, core: 2. Of those that a mesh axis runs over, the one named last changes fastest.
Arguments:
- queries: bfloat16 [1024, 1024], P('sp', 'tp'), may hold values from -12 to 12
- keys: bfloat16 [1024, 256], P('sp', 'tp'), may hold values from -12 to 12
- values: bfloat16 [1024, 256], P('sp', 'tp'), may hold values from -6 to 6
- log_gate: float32 [16, 1024], P('tp', 'sp'), may hold values from -0.2 to 0, as said below
- log_sum: float32 [16, 1024], P('tp', 'sp'), may hold values from -100 to 100, as said below
- output: bfloat16 [1024, 1024], P('sp', 'tp'), may hold values from -6 to 6
- cotangent: bfloat16 [1024, 1024], P('sp', 'tp'), may hold values from -12 to 12
- normed: bfloat16 [1024, 2048], P('sp', 'tp'), may hold values from -8 to 8
Outputs:
- query_grad: bfloat16 [1024, 1024], P('sp', 'tp')
- key_grad: bfloat16 [1024, 256], P('sp', 'tp')
- value_grad: bfloat16 [1024, 256], P('sp', 'tp')
- weight_grad: float32 [2048, 256], P('sp', 'tp')
Inputs may be any that keep to these rules, and one draw needn't show every extreme that they name: `log_gate`: every entry is negative. log_sum[h, t] is the logarithm of the sum over s <= t of exp of the scores of the steps (before log_sum is subtracted), computed from the given queries, keys and log_gate.
All inputs are finite; a program needn't handle non-finite values.
Results may differ from a plain program's by a relative error of at most 0.005.
Values may be sent and summed in bfloat16 or wider, within the bound.
A program may use at most 64 MiB of HBM per device.

v0:
```python
import jax
import jax.numpy as jnp
from jax import lax
from jax.sharding import PartitionSpec as P

HDIM = 64
NEG_LARGE = -1e30


def prefix(x, axis, combine, identity):
    size, place = (lax.axis_size(axis), lax.axis_index(axis))
    everything = lax.all_gather(x, axis)
    start = jnp.broadcast_to(jnp.asarray(identity, x.dtype), x.shape)

    def hop(k, before):
        reached = k < place
        new = combine(before, everything[k])
        return jnp.where(reached, new, before)

    return lax.fori_loop(0, size, hop, start)


def shifted(x, axis, by):
    size = lax.axis_size(axis)
    pairs = [(i, i + by) for i in range(size) if 0 <= i + by < size]
    return lax.ppermute(x, axis, pairs)


def shifted_2(x, axis, by):
    size = lax.axis_size(axis)
    return lax.ppermute(x, axis, [(i, (i + by) % size) for i in range(size)])


def add_pair(earlier, later):
    return earlier + later


def body(queries, keys, values, log_gate, log_sum, output, cotangent, normed):
    tokens = queries.shape[0]
    head_count = log_gate.shape[0]
    kv_width = keys.shape[1]
    kv_heads = kv_width // HDIM
    groups = head_count // kv_heads
    inverse_root = HDIM ** (-0.5)
    devices = lax.axis_size("sp")
    my_index = lax.axis_index("sp")
    depth = 8
    totals = jnp.sum(log_gate, axis=1)
    before = prefix(totals, "sp", add_pair, jnp.zeros_like(totals))
    cumulative = jnp.cumsum(log_gate, axis=1) + before[:, None]
    row_terms = jnp.sum(
        (output.astype(jnp.float32) * cotangent.astype(jnp.float32)).reshape(
            tokens, head_count, HDIM
        ),
        axis=2,
    ).T
    query_split = queries.reshape(tokens, kv_heads, groups, HDIM)
    cotan_split = cotangent.reshape(tokens, kv_heads, groups, HDIM)
    cum_rows = cumulative.reshape(kv_heads, groups, tokens)
    lse_rows = log_sum.reshape(kv_heads, groups, tokens)
    term_rows = row_terms.reshape(kv_heads, groups, tokens)
    positions = my_index * tokens + jnp.arange(tokens)
    last_row = my_index * tokens + tokens - 1

    def visit_bundle(bundle, bundle_cum, key_pos):
        count = bundle.shape[0]
        block_rows = bundle.shape[1]
        key_rows = count * block_rows
        flat = bundle.reshape(key_rows, 2 * kv_width)
        flat_cum = jnp.transpose(bundle_cum, (1, 0, 2)).reshape(kv_heads, groups, key_rows)
        flat_pos = key_pos.reshape(key_rows)
        key_part = flat[:, :kv_width].reshape(key_rows, kv_heads, HDIM)
        value_part = flat[:, kv_width:].reshape(key_rows, kv_heads, HDIM)

        def attend(unused):
            scores = (
                jnp.einsum(
                    "qhgd,khd->hgqk", query_split, key_part, preferred_element_type=jnp.float32
                )
                * inverse_root
            )
            scores = (
                scores + cum_rows[:, :, :, None] - flat_cum[:, :, None, :] - lse_rows[:, :, :, None]
            )
            allowed = flat_pos[None, :] <= positions[:, None]
            weights = jnp.exp(jnp.where(allowed, scores, NEG_LARGE))
            upstream = jnp.einsum(
                "qhgd,khd->hgqk", cotan_split, value_part, preferred_element_type=jnp.float32
            )
            dscore_low = (weights * (upstream - term_rows[:, :, :, None])).astype(jnp.bfloat16)
            weights_low = weights.astype(jnp.bfloat16)
            query_add = (
                jnp.einsum(
                    "hgqk,khd->qhgd", dscore_low, key_part, preferred_element_type=jnp.float32
                )
                * inverse_root
            )
            key_add = (
                jnp.einsum(
                    "hgqk,qhgd->khd", dscore_low, query_split, preferred_element_type=jnp.float32
                )
                * inverse_root
            )
            value_add = jnp.einsum(
                "hgqk,qhgd->khd", weights_low, cotan_split, preferred_element_type=jnp.float32
            )
            joined = jnp.concatenate(
                [key_add.reshape(key_rows, kv_width), value_add.reshape(key_rows, kv_width)], axis=1
            )
            return (query_add, joined.reshape(count, block_rows, 2 * kv_width))

        def nothing(unused):
            return (
                jnp.zeros((tokens, kv_heads, groups, HDIM), jnp.float32),
                jnp.zeros((count, block_rows, 2 * kv_width), jnp.float32),
            )

        return lax.cond(jnp.min(flat_pos) <= last_row, attend, nothing, 0)

    stacked = jnp.concatenate([keys, values], axis=1)
    query_start = jnp.zeros((tokens, kv_heads, groups, HDIM), jnp.float32)
    copies = jnp.arange(depth)
    turns = devices // depth
    bundle_pieces = [stacked]
    bundle_cums = [cumulative]
    for step in range(1, depth):
        bundle_pieces.append(shifted(stacked, "sp", step))
        bundle_cums.append(shifted(cumulative, "sp", step))

    def turn(turn_index, state_now):
        query_total, bundle, bundle_cum, bundle_grads = state_now
        anchor = (my_index - depth * turn_index) % devices
        blocks = (anchor - copies) % devices
        key_pos = blocks[:, None] * tokens + jnp.arange(tokens)[None, :]
        query_add, grad_add = visit_bundle(bundle, bundle_cum, key_pos)
        bundle = shifted(bundle, "sp", depth)
        bundle_cum, bundle_grads = shifted_2((bundle_cum, bundle_grads + grad_add), "sp", depth)
        return (query_total + query_add, bundle, bundle_cum, bundle_grads)

    start_state = (
        query_start,
        jnp.stack(bundle_pieces),
        jnp.stack(bundle_cums),
        jnp.zeros((depth, tokens, 2 * kv_width), jnp.float32),
    )
    finished = lax.fori_loop(0, turns, turn, start_state)
    query_total = finished[0]
    final_grads = finished[3]
    gradients = final_grads[0]
    for step in range(1, depth):
        gradients = gradients + shifted(final_grads[step], "sp", -step)
    query_grad = query_total.reshape(tokens, head_count * HDIM).astype(jnp.bfloat16)
    key_grad = gradients[:, :kv_width].astype(jnp.bfloat16)
    value_grad = gradients[:, kv_width:].astype(jnp.bfloat16)
    whole_rows = lax.all_gather(normed, "tp", axis=1, tiled=True)
    weight_grad = lax.psum_scatter(
        lax.dot_general(
            whole_rows, key_grad, (((0,), (0,)), ((), ())), preferred_element_type=jnp.float32
        ),
        "sp",
        scatter_dimension=0,
        tiled=True,
    )
    return (query_grad, key_grad, value_grad, weight_grad)


def solution(mesh):
    in_specs = (
        P("sp", "tp"),
        P("sp", "tp"),
        P("sp", "tp"),
        P("tp", "sp"),
        P("tp", "sp"),
        P("sp", "tp"),
        P("sp", "tp"),
        P("sp", "tp"),
    )
    out_specs = (P("sp", "tp"), P("sp", "tp"), P("sp", "tp"), P("sp", "tp"))
    return jax.shard_map(body, mesh=mesh, in_specs=in_specs, out_specs=out_specs, check_vma=False)
```

profile of v0, /device:TPU:0, one launch (start us, length us, event | category | flops | bytes accessed | tf_op | source)
XLA Modules:
  0.0 176.8 jit_solution(9886937687388479770)
XLA Ops:
  11.2 23.1 %all-reduce = f32[32]{0:T(128)S(1)} all-reduce(f32[32]{0:T(128)S(1)} %dynamic-update-slice), channel_id=2, replica_groups=mesh['sp'=8,'tp'=4] {'sp'}, use_global_device_ids=true, to_apply=%add | all-reduce | flops 32 | bytes 256
  34.7 1.6 collective-permute-start.13
  40.3 2.5 %collective-permute-start.7 = (f32[4,128]{1,0:T(4,128)S(1)}, f32[4,128]{1,0:T(4,128)S(1)}, u32[]{:S(2)}, u32[]{:S(2)}) collective-permute-start(f32[4,128]{1,0:T(4,128)S(1)} %broadcast_add_fusion.1), channel_id=1, source_target_pairs={{0,4},{4,8},{8,12},{12,16},{16,20},{20,24},{24,28},{1,5},{5,9},{9,... | collective-permute-start | bytes 6152 | tf_op jit(solution)/shard_map/ppermute | solution.py:26
  47.9 2.5 %collective-permute-start.8 = (f32[4,128]{1,0:T(4,128)S(1)}, f32[4,128]{1,0:T(4,128)S(1)}, u32[]{:S(2)}, u32[]{:S(2)}) collective-permute-start(f32[4,128]{1,0:T(4,128)S(1)} %broadcast_add_fusion.1), channel_id=1, source_target_pairs={{0,8},{4,12},{8,16},{12,20},{16,24},{20,28},{1,9},{5,13},{9,17},{1... | collective-permute-start | bytes 6152 | tf_op jit(solution)/shard_map/ppermute | solution.py:26
  51.7 3.9 %collective-permute-start.9 = (f32[4,128]{1,0:T(4,128)S(1)}, f32[4,128]{1,0:T(4,128)S(1)}, u32[]{:S(2)}, u32[]{:S(2)}) collective-permute-start(f32[4,128]{1,0:T(4,128)S(1)} %broadcast_add_fusion.1), channel_id=1, source_target_pairs={{0,12},{4,16},{8,20},{12,24},{16,28},{1,13},{5,17},{9,21},{13,25},... | collective-permute-start | bytes 6152 | tf_op jit(solution)/shard_map/ppermute | solution.py:26
  56.9 5.1 %collective-permute-start.5 = (bf16[128,128]{1,0:T(8,128)(2,1)S(1)}, bf16[128,128]{1,0:T(8,128)(2,1)S(1)}, u32[]{:S(2)}, u32[]{:S(2)}) collective-permute-start(bf16[128,128]{1,0:T(8,128)(2,1)S(1)} %get-tuple-element.251), channel_id=1, source_target_pairs={{0,24},{4,28},{1,25},{5,29},{2,26},{6,30},{3,27},{7,31}} | collective-permute-start | bytes 98312 | tf_op jit(solution)/shard_map/ppermute | solution.py:26
  64.6 1.6 collective-permute-start.2
  66.3 3.0 %collective-permute-start = (bf16[128,128]{1,0:T(8,128)(2,1)S(1)}, bf16[128,128]{1,0:T(8,128)(2,1)S(1)}, u32[]{:S(2)}, u32[]{:S(2)}) collective-permute-start(bf16[128,128]{1,0:T(8,128)(2,1)S(1)} %get-tuple-element.251), channel_id=1, source_target_pairs={{0,4},{4,8},{8,12},{12,16},{16,20},{20,24},{24,28},{1,5},{5,9},{9,... | collective-permute-start | bytes 98312 | tf_op jit(solution)/shard_map/ppermute | solution.py:26
  69.3 1.6 collective-permute-done
  70.9 4.2 %collective-permute-start.1 = (bf16[128,128]{1,0:T(8,128)(2,1)S(1)}, bf16[128,128]{1,0:T(8,128)(2,1)S(1)}, u32[]{:S(2)}, u32[]{:S(2)}) collective-permute-start(bf16[128,128]{1,0:T(8,128)(2,1)S(1)} %get-tuple-element.251), channel_id=1, source_target_pairs={{0,8},{4,12},{8,16},{12,20},{16,24},{20,28},{1,9},{5,13},{9,17},{1... | collective-permute-start | bytes 98312 | tf_op jit(solution)/shard_map/ppermute | solution.py:26
  75.1 1.6 collective-permute-done.1
  76.7 1.6 collective-permute-start.6
  78.4 1.5 collective-permute-done.6
  79.9 5.7 %conditional.1 = (f32[8,128,128]{1,2,0:T(8,128)S(1)}, bf16[128,256]{1,0:T(8,128)(2,1)S(1)}) conditional(s32[]{:T(128)} %convert_element_type.39, () %tuple.37, (s32[8,128]{1,0:T(8,128)S(1)}, s32[]{:T(128)}, s32[128]{0:T(128)S(1)}, bf16[8,128,128]{2,1,0:T(8,128)(2,1)S(1)}, bf16[128,256]{1,0:T(8,128)(2,1)}, /*index=5*/f32[4,128]{1,0:T(4,128)S(1)}, ...), branch_computations={%region_6.7_spmd, %region_7.8_spmd} | conditional | flops 340656256 | bytes 13856276 | solution.py:118
  82.1 1.5 fusion.21
  85.7 1.3 collective-permute-start.15
  87.0 1.3 collective-permute-start.21
  88.3 1.3 collective-permute-start.20
  89.6 1.3 collective-permute-start.19
  90.9 1.3 collective-permute-start.18
  92.2 1.3 collective-permute-start.17
  93.5 2.3 %collective-permute-done.21 = f32[128,128]{0,1:T(8,128)S(1)} collective-permute-done((f32[128,128]{0,1:T(8,128)S(1)}, f32[128,128]{0,1:T(8,128)S(1)}, u32[]{:S(2)}, u32[]{:S(2)}) %collective-permute-start.21) | collective-permute-done | bytes 65568 | tf_op jit(solution)/shard_map/ppermute | solution.py:26
  97.1 7.2 %all_gather.11 = bf16[128,2048]{1,0:T(8,128)(2,1)S(1)} all-gather(bf16[128,512]{1,0:T(8,128)(2,1)S(1)} %copy-done), channel_id=1, replica_groups=mesh['sp'=8,'tp'=4] {'tp'}, dimensions={1}, use_global_device_ids=true | all-gather | bytes 655360 | tf_op jit(solution)/shard_map/all_gather | solution.py:155
  106.1 63.9 %reduce-scatter.2.cloned.1.call-done = f32[256,64]{0,1:T(8,128)} async-done(((f32[2048,64]{0,1:T(8,128)}), f32[256,64]{0,1:T(8,128)}) %reduce-scatter.2.cloned.1.call-update) | async-done | bytes 65552 | tf_op jit(solution)/shard_map/reduce_scatter | solution.py:156
  (90 shorter events, 24.7 us)
Async XLA Ops:
  7.2 162.8 %reduce-scatter.2.cloned.1.call-start = ((), (), s32[]{:S(2)}) async-start(), calls=%async_computation.1 | async-start | bytes 589824 | tf_op jit(solution)/shard_map/reduce_scatter | solution.py:156
  34.7 31.6 %collective-permute-start.13 = (f32[4,128]{1,0:T(4,128)S(1)}, f32[4,128]{1,0:T(4,128)S(1)}, u32[]{:S(2)}, u32[]{:S(2)}) collective-permute-start(f32[4,128]{1,0:T(4,128)S(1)} %broadcast_add_fusion.1), channel_id=1, source_target_pairs={{0,28},{1,29},{2,30},{3,31}} | collective-permute-start | bytes 6152 | tf_op jit(solution)/shard_map/ppermute | solution.py:26
  36.4 28.2 %collective-permute-start.12 = (f32[4,128]{1,0:T(4,128)S(1)}, f32[4,128]{1,0:T(4,128)S(1)}, u32[]{:S(2)}, u32[]{:S(2)}) collective-permute-start(f32[4,128]{1,0:T(4,128)S(1)} %broadcast_add_fusion.1), channel_id=1, source_target_pairs={{0,24},{4,28},{1,25},{5,29},{2,26},{6,30},{3,27},{7,31}} | collective-permute-start | bytes 6152 | tf_op jit(solution)/shard_map/ppermute | solution.py:26
  37.7 25.6 %collective-permute-start.11 = (f32[4,128]{1,0:T(4,128)S(1)}, f32[4,128]{1,0:T(4,128)S(1)}, u32[]{:S(2)}, u32[]{:S(2)}) collective-permute-start(f32[4,128]{1,0:T(4,128)S(1)} %broadcast_add_fusion.1), channel_id=1, source_target_pairs={{0,20},{4,24},{8,28},{1,21},{5,25},{9,29},{2,22},{6,26},{10,30},{3... | collective-permute-start | bytes 6152 | tf_op jit(solution)/shard_map/ppermute | solution.py:26
  39.0 23.0 %collective-permute-start.10 = (f32[4,128]{1,0:T(4,128)S(1)}, f32[4,128]{1,0:T(4,128)S(1)}, u32[]{:S(2)}, u32[]{:S(2)}) collective-permute-start(f32[4,128]{1,0:T(4,128)S(1)} %broadcast_add_fusion.1), channel_id=1, source_target_pairs={{0,16},{4,20},{8,24},{12,28},{1,17},{5,21},{9,25},{13,29},{2,18},{... | collective-permute-start | bytes 6152 | tf_op jit(solution)/shard_map/ppermute | solution.py:26
  40.3 7.6 %collective-permute-start.7 = (f32[4,128]{1,0:T(4,128)S(1)}, f32[4,128]{1,0:T(4,128)S(1)}, u32[]{:S(2)}, u32[]{:S(2)}) collective-permute-start(f32[4,128]{1,0:T(4,128)S(1)} %broadcast_add_fusion.1), channel_id=1, source_target_pairs={{0,4},{4,8},{8,12},{12,16},{16,20},{20,24},{24,28},{1,5},{5,9},{9,... | collective-permute-start | bytes 6152 | tf_op jit(solution)/shard_map/ppermute | solution.py:26
  47.9 3.8 %collective-permute-start.8 = (f32[4,128]{1,0:T(4,128)S(1)}, f32[4,128]{1,0:T(4,128)S(1)}, u32[]{:S(2)}, u32[]{:S(2)}) collective-permute-start(f32[4,128]{1,0:T(4,128)S(1)} %broadcast_add_fusion.1), channel_id=1, source_target_pairs={{0,8},{4,12},{8,16},{12,20},{16,24},{20,28},{1,9},{5,13},{9,17},{1... | collective-permute-start | bytes 6152 | tf_op jit(solution)/shard_map/ppermute | solution.py:26
  51.7 5.2 %collective-permute-start.9 = (f32[4,128]{1,0:T(4,128)S(1)}, f32[4,128]{1,0:T(4,128)S(1)}, u32[]{:S(2)}, u32[]{:S(2)}) collective-permute-start(f32[4,128]{1,0:T(4,128)S(1)} %broadcast_add_fusion.1), channel_id=1, source_target_pairs={{0,12},{4,16},{8,20},{12,24},{16,28},{1,13},{5,17},{9,21},{13,25},... | collective-permute-start | bytes 6152 | tf_op jit(solution)/shard_map/ppermute | solution.py:26
  56.9 21.5 %collective-permute-start.5 = (bf16[128,128]{1,0:T(8,128)(2,1)S(1)}, bf16[128,128]{1,0:T(8,128)(2,1)S(1)}, u32[]{:S(2)}, u32[]{:S(2)}) collective-permute-start(bf16[128,128]{1,0:T(8,128)(2,1)S(1)} %get-tuple-element.251), channel_id=1, source_target_pairs={{0,24},{4,28},{1,25},{5,29},{2,26},{6,30},{3,27},{7,31}} | collective-permute-start | bytes 98312 | tf_op jit(solution)/shard_map/ppermute | solution.py:26
  62.0 16.4 %collective-permute-start.4 = (bf16[128,128]{1,0:T(8,128)(2,1)S(1)}, bf16[128,128]{1,0:T(8,128)(2,1)S(1)}, u32[]{:S(2)}, u32[]{:S(2)}) collective-permute-start(bf16[128,128]{1,0:T(8,128)(2,1)S(1)} %get-tuple-element.251), channel_id=1, source_target_pairs={{0,20},{4,24},{8,28},{1,21},{5,25},{9,29},{2,22},{6,26},{10,30},{3... | collective-permute-start | bytes 98312 | tf_op jit(solution)/shard_map/ppermute | solution.py:26
  63.3 15.0 %collective-permute-start.3 = (bf16[128,128]{1,0:T(8,128)(2,1)S(1)}, bf16[128,128]{1,0:T(8,128)(2,1)S(1)}, u32[]{:S(2)}, u32[]{:S(2)}) collective-permute-start(bf16[128,128]{1,0:T(8,128)(2,1)S(1)} %get-tuple-element.251), channel_id=1, source_target_pairs={{0,16},{4,20},{8,24},{12,28},{1,17},{5,21},{9,25},{13,29},{2,18},{... | collective-permute-start | bytes 98312 | tf_op jit(solution)/shard_map/ppermute | solution.py:26
  64.6 13.7 %collective-permute-start.2 = (bf16[128,128]{1,0:T(8,128)(2,1)S(1)}, bf16[128,128]{1,0:T(8,128)(2,1)S(1)}, u32[]{:S(2)}, u32[]{:S(2)}) collective-permute-start(bf16[128,128]{1,0:T(8,128)(2,1)S(1)} %get-tuple-element.251), channel_id=1, source_target_pairs={{0,12},{4,16},{8,20},{12,24},{16,28},{1,13},{5,17},{9,21},{13,25},... | collective-permute-start | bytes 98312 | tf_op jit(solution)/shard_map/ppermute | solution.py:26
  66.3 4.6 %collective-permute-start = (bf16[128,128]{1,0:T(8,128)(2,1)S(1)}, bf16[128,128]{1,0:T(8,128)(2,1)S(1)}, u32[]{:S(2)}, u32[]{:S(2)}) collective-permute-start(bf16[128,128]{1,0:T(8,128)(2,1)S(1)} %get-tuple-element.251), channel_id=1, source_target_pairs={{0,4},{4,8},{8,12},{12,16},{16,20},{20,24},{24,28},{1,5},{5,9},{9,... | collective-permute-start | bytes 98312 | tf_op jit(solution)/shard_map/ppermute | solution.py:26
  70.9 5.8 %collective-permute-start.1 = (bf16[128,128]{1,0:T(8,128)(2,1)S(1)}, bf16[128,128]{1,0:T(8,128)(2,1)S(1)}, u32[]{:S(2)}, u32[]{:S(2)}) collective-permute-start(bf16[128,128]{1,0:T(8,128)(2,1)S(1)} %get-tuple-element.251), channel_id=1, source_target_pairs={{0,8},{4,12},{8,16},{12,20},{16,24},{20,28},{1,9},{5,13},{9,17},{1... | collective-permute-start | bytes 98312 | tf_op jit(solution)/shard_map/ppermute | solution.py:26
  76.7 3.2 %collective-permute-start.6 = (bf16[128,128]{1,0:T(8,128)(2,1)S(1)}, bf16[128,128]{1,0:T(8,128)(2,1)S(1)}, u32[]{:S(2)}, u32[]{:S(2)}) collective-permute-start(bf16[128,128]{1,0:T(8,128)(2,1)S(1)} %get-tuple-element.251), channel_id=1, source_target_pairs={{0,28},{1,29},{2,30},{3,31}} | collective-permute-start | bytes 98312 | tf_op jit(solution)/shard_map/ppermute | solution.py:26
  85.5 84.4 %copy-start.2 = (bf16[128,256]{1,0:T(8,128)(2,1)}, bf16[128,256]{1,0:T(8,128)(2,1)S(1)}, u32[]{:S(2)}) copy-start(bf16[128,256]{1,0:T(8,128)(2,1)S(1)} %get-tuple-element.241) | copy-start | bytes 196612
  85.7 6.5 %collective-permute-start.15 = (f32[128,128]{0,1:T(8,128)S(1)}, f32[128,128]{0,1:T(8,128)S(1)}, u32[]{:S(2)}, u32[]{:S(2)}) collective-permute-start(f32[128,128]{0,1:T(8,128)S(1)} %get-tuple-element.254), channel_id=1, source_target_pairs={{4,0},{8,4},{12,8},{16,12},{20,16},{24,20},{28,24},{5,1},{9,5},{13... | collective-permute-start | bytes 196616 | tf_op jit(solution)/shard_map/ppermute | solution.py:26
  87.0 8.9 %collective-permute-start.21 = (f32[128,128]{0,1:T(8,128)S(1)}, f32[128,128]{0,1:T(8,128)S(1)}, u32[]{:S(2)}, u32[]{:S(2)}) collective-permute-start(f32[128,128]{0,1:T(8,128)S(1)} %get-tuple-element.255), channel_id=1, source_target_pairs={{28,0},{29,1},{30,2},{31,3}} | collective-permute-start | bytes 196616 | tf_op jit(solution)/shard_map/ppermute | solution.py:26
  88.3 16.1 %collective-permute-start.20 = (f32[128,128]{0,1:T(8,128)S(1)}, f32[128,128]{0,1:T(8,128)S(1)}, u32[]{:S(2)}, u32[]{:S(2)}) collective-permute-start(f32[128,128]{0,1:T(8,128)S(1)} %get-tuple-element.256), channel_id=1, source_target_pairs={{24,0},{28,4},{25,1},{29,5},{26,2},{30,6},{27,3},{31,7}} | collective-permute-start | bytes 196616 | tf_op jit(solution)/shard_map/ppermute | solution.py:26
  89.6 14.8 %collective-permute-start.19 = (f32[128,128]{0,1:T(8,128)S(1)}, f32[128,128]{0,1:T(8,128)S(1)}, u32[]{:S(2)}, u32[]{:S(2)}) collective-permute-start(f32[128,128]{0,1:T(8,128)S(1)} %get-tuple-element.257), channel_id=1, source_target_pairs={{20,0},{24,4},{28,8},{21,1},{25,5},{29,9},{22,2},{26,6},{30,10},{2... | collective-permute-start | bytes 196616 | tf_op jit(solution)/shard_map/ppermute | solution.py:26
  90.9 13.5 %collective-permute-start.18 = (f32[128,128]{0,1:T(8,128)S(1)}, f32[128,128]{0,1:T(8,128)S(1)}, u32[]{:S(2)}, u32[]{:S(2)}) collective-permute-start(f32[128,128]{0,1:T(8,128)S(1)} %get-tuple-element.258), channel_id=1, source_target_pairs={{16,0},{20,4},{24,8},{28,12},{17,1},{21,5},{25,9},{29,13},{18,2},{... | collective-permute-start | bytes 196616 | tf_op jit(solution)/shard_map/ppermute | solution.py:26
  92.2 12.2 %collective-permute-start.17 = (f32[128,128]{0,1:T(8,128)S(1)}, f32[128,128]{0,1:T(8,128)S(1)}, u32[]{:S(2)}, u32[]{:S(2)}) collective-permute-start(f32[128,128]{0,1:T(8,128)S(1)} %get-tuple-element.259), channel_id=1, source_target_pairs={{12,0},{16,4},{20,8},{24,12},{28,16},{13,1},{17,5},{21,9},{25,13},... | collective-permute-start | bytes 196616 | tf_op jit(solution)/shard_map/ppermute | solution.py:26
  95.8 8.5 %collective-permute-start.16 = (f32[128,128]{0,1:T(8,128)S(1)}, f32[128,128]{0,1:T(8,128)S(1)}, u32[]{:S(2)}, u32[]{:S(2)}) collective-permute-start(f32[128,128]{0,1:T(8,128)S(1)} %get-tuple-element.260), channel_id=1, source_target_pairs={{8,0},{12,4},{16,8},{20,12},{24,16},{28,20},{9,1},{13,5},{17,9},{2... | collective-permute-start | bytes 196616 | tf_op jit(solution)/shard_map/ppermute | solution.py:26
  105.0 65.0 %copy-start.1 = (bf16[128,64]{0,1:T(8,128)(2,1)}, bf16[128,64]{0,1:T(8,128)(2,1)S(1)}, u32[]{:S(2)}) copy-start(bf16[128,64]{0,1:T(8,128)(2,1)S(1)} %get-tuple-element.262) | copy-start | bytes 49156
  (2 other events, 17.3 us)
Sparse Core Ops, SparseCore 0:
  106.2 63.7 reduce-scatter.1
where the time goes:
time: 178 us; the launch traced here: 177 us
  waiting for transfers between devices  73.4 us (41%)
  starting transfers between devices  41.6 us (23%)
  blocking collectives  30.3 us (17%)
  between operations  15.8 us (9%)
  local copies, waits for them, and re-layouts  8.07 us (5%)
  matrix products  4.19 us (2%)
  other arithmetic  3.18 us (2%)
    reduce_scatter x1, waiting for transfers between devices, body(): lax.psum_scatter(lax.dot_general(whole_rows, key_grad, (((0,), (0,)), (()...  63.9 us
    ppermute x21, starting transfers between devices, shifted(): return lax.ppermute(x, axis, pairs)  41.5 us
    unnamed x1, blocking collectives  23.1 us
    ppermute x21, waiting for transfers between devices, shifted(): return lax.ppermute(x, axis, pairs)  9.53 us
    all_gather x1, blocking collectives, body(): whole_rows = lax.all_gather(normed, 'tp', axis=1, tiled=True)  7.21 us
    unnamed x25, local copies, waits for them, and re-layouts  5.18 us
  transfers between devices with their start and end apart: 23, of which 7 were waited for; matrix products, arithmetic and copies ran while one was open for 3% of the time, Pallas kernels for 0%

commit v1 on v0

--- a/solution.py
+++ b/solution.py
@@ -1,3 +1,4 @@
+import functools
 import jax
 import jax.numpy as jnp
 from jax import lax
@@ -5,6 +6,17 @@
 
 HDIM = 64
 NEG_LARGE = -1e30
+
+
+def run_the_streams(block_in, shard_axis):
+    wide_out = jnp.concatenate(
+        jax.lax.all_to_all(jnp.stack([block_in] * jax.lax.axis_size(shard_axis)), shard_axis, 0, 0),
+        axis=1,
+    )
+    return wide_out
+
+
+update_tails_by_axis = functools.partial(run_the_streams, shard_axis="tp")
 
 
 def prefix(x, axis, combine, identity):
@@ -152,7 +164,7 @@
     query_grad = query_total.reshape(tokens, head_count * HDIM).astype(jnp.bfloat16)
     key_grad = gradients[:, :kv_width].astype(jnp.bfloat16)
     value_grad = gradients[:, kv_width:].astype(jnp.bfloat16)
-    whole_rows = lax.all_gather(normed, "tp", axis=1, tiled=True)
+    whole_rows = update_tails_by_axis(normed)
     weight_grad = lax.psum_scatter(
         lax.dot_general(
             whole_rows, key_grad, (((0,), (0,)), ((), ())), preferred_element_type=jnp.float32

time: 178 us -> 206 us (1.16)
  starting transfers between devices: 41.6 us -> 69.2 us
  blocking collectives: 30.3 us -> 17.9 us
  waiting for transfers between devices: 73.4 us -> 84.6 us
    ppermute x21, starting transfers between devices: 41.5 us -> 64.6 us  [shifted(): return lax.ppermute(x, axis, pairs)]
    all_to_all x0 -> x1, waiting for transfers between devices: none -> 8.03 us  [run_the_streams(): jax.lax.all_to_all(jnp.stack([block_in] * jax.lax.axis_size(shard_axis)),...]
    all_gather x1 -> x0, blocking collectives: 7.21 us -> none  [body(): whole_rows = lax.all_gather(normed, 'tp', axis=1, tiled=True)]
    unnamed x1, blocking collectives: 23.1 us -> 17.9 us
    all_to_all x0 -> x1, starting transfers between devices: none -> 3.47 us  [run_the_streams(): jax.lax.all_to_all(jnp.stack([block_in] * jax.lax.axis_size(shard_axis)),...]
    unnamed x25 -> x24, local copies, waits for them, and re-layouts: 5.18 us -> 6.19 us
  transfers between devices with their start and end apart: 23 -> 24, of which waited for: 7 -> 10; matrix products, arithmetic and copies ran while one was open for 3% -> 4% of each run, Pallas kernels for 0% -> 0%
where the time goes in v1:
time: 206 us; the launch traced here: 205 us
  waiting for transfers between devices  84.6 us (41%)
  starting transfers between devices  69.2 us (34%)
  blocking collectives  17.9 us (9%)
  between operations  15.8 us (8%)
  local copies, waits for them, and re-layouts  9.1 us (4%)
  matrix products  4.35 us (2%)
  other arithmetic  3.99 us (2%)
    reduce_scatter x1, waiting for transfers between devices, body(): lax.psum_scatter(lax.dot_general(whole_rows, key_grad, (((0,), (0,)), (()...  65 us
    ppermute x21, starting transfers between devices, shifted(): return lax.ppermute(x, axis, pairs)  64.6 us
    unnamed x1, blocking collectives  17.9 us
    ppermute x21, waiting for transfers between devices, shifted(): return lax.ppermute(x, axis, pairs)  11.5 us
    all_to_all x1, waiting for transfers between devices, run_the_streams(): jax.lax.all_to_all(jnp.stack([block_in] * jax.lax.axis_size(shard_axis)),...  8.03 us
    unnamed x24, local copies, waits for them, and re-layouts  6.19 us
  transfers between devices with their start and end apart: 24, of which 10 were waited for; matrix products, arithmetic and copies ran while one was open for 4% of the time, Pallas kernels for 0%

profile of v1, /device:TPU:0, one launch (start us, length us, event | category | flops | bytes accessed | tf_op | source)
XLA Modules:
  0.0 205.2 jit_solution(13457727629967190589)
XLA Ops:
  8.9 4.9 %collective-permute-start = (bf16[128,128]{1,0:T(8,128)(2,1)S(1)}, bf16[128,128]{1,0:T(8,128)(2,1)S(1)}, u32[]{:S(2)}, u32[]{:S(2)}) collective-permute-start(bf16[128,128]{1,0:T(8,128)(2,1)S(1)} %get-tuple-element.251), channel_id=1, source_target_pairs={{0,4},{4,8},{8,12},{12,16},{16,20},{20,24},{24,28},{1,5},{5,9},{9,... | collective-permute-start | bytes 98312 | tf_op jit(solution)/shard_map/ppermute | solution.py:38
  13.8 3.5 %collective-permute-start.1 = (bf16[128,128]{1,0:T(8,128)(2,1)S(1)}, bf16[128,128]{1,0:T(8,128)(2,1)S(1)}, u32[]{:S(2)}, u32[]{:S(2)}) collective-permute-start(bf16[128,128]{1,0:T(8,128)(2,1)S(1)} %get-tuple-element.251), channel_id=1, source_target_pairs={{0,8},{4,12},{8,16},{12,20},{16,24},{20,28},{1,9},{5,13},{9,17},{1... | collective-permute-start | bytes 98312 | tf_op jit(solution)/shard_map/ppermute | solution.py:38
  17.3 4.5 %collective-permute-start.2 = (bf16[128,128]{1,0:T(8,128)(2,1)S(1)}, bf16[128,128]{1,0:T(8,128)(2,1)S(1)}, u32[]{:S(2)}, u32[]{:S(2)}) collective-permute-start(bf16[128,128]{1,0:T(8,128)(2,1)S(1)} %get-tuple-element.251), channel_id=1, source_target_pairs={{0,12},{4,16},{8,20},{12,24},{16,28},{1,13},{5,17},{9,21},{13,25},... | collective-permute-start | bytes 98312 | tf_op jit(solution)/shard_map/ppermute | solution.py:38
  21.8 1.9 collective-permute-start.3
  27.7 17.9 %all-reduce = f32[32]{0:T(128)S(1)} all-reduce(f32[32]{0:T(128)S(1)} %dynamic-update-slice), channel_id=2, replica_groups=mesh['sp'=8,'tp'=4] {'sp'}, use_global_device_ids=true, to_apply=%add | all-reduce | flops 32 | bytes 256
  46.1 3.1 %collective-permute-start.7 = (f32[4,128]{1,0:T(4,128)S(1)}, f32[4,128]{1,0:T(4,128)S(1)}, u32[]{:S(2)}, u32[]{:S(2)}) collective-permute-start(f32[4,128]{1,0:T(4,128)S(1)} %broadcast_add_fusion.1), channel_id=1, source_target_pairs={{0,4},{4,8},{8,12},{12,16},{16,20},{20,24},{24,28},{1,5},{5,9},{9,... | collective-permute-start | bytes 6152 | tf_op jit(solution)/shard_map/ppermute | solution.py:38
  52.6 1.5 collective-permute-start.8
  55.4 3.5 %collective-permute-start.9 = (f32[4,128]{1,0:T(4,128)S(1)}, f32[4,128]{1,0:T(4,128)S(1)}, u32[]{:S(2)}, u32[]{:S(2)}) collective-permute-start(f32[4,128]{1,0:T(4,128)S(1)} %broadcast_add_fusion.1), channel_id=1, source_target_pairs={{0,12},{4,16},{8,20},{12,24},{16,28},{1,13},{5,17},{9,21},{13,25},... | collective-permute-start | bytes 6152 | tf_op jit(solution)/shard_map/ppermute | solution.py:38
  60.2 6.0 %collective-permute-start.10 = (f32[4,128]{1,0:T(4,128)S(1)}, f32[4,128]{1,0:T(4,128)S(1)}, u32[]{:S(2)}, u32[]{:S(2)}) collective-permute-start(f32[4,128]{1,0:T(4,128)S(1)} %broadcast_add_fusion.1), channel_id=1, source_target_pairs={{0,16},{4,20},{8,24},{12,28},{1,17},{5,21},{9,25},{13,29},{2,18},{... | collective-permute-start | bytes 6152 | tf_op jit(solution)/shard_map/ppermute | solution.py:38
  67.5 4.9 %collective-permute-start.11 = (f32[4,128]{1,0:T(4,128)S(1)}, f32[4,128]{1,0:T(4,128)S(1)}, u32[]{:S(2)}, u32[]{:S(2)}) collective-permute-start(f32[4,128]{1,0:T(4,128)S(1)} %broadcast_add_fusion.1), channel_id=1, source_target_pairs={{0,20},{4,24},{8,28},{1,21},{5,25},{9,29},{2,22},{6,26},{10,30},{3... | collective-permute-start | bytes 6152 | tf_op jit(solution)/shard_map/ppermute | solution.py:38
  73.7 8.6 %collective-permute-start.12 = (f32[4,128]{1,0:T(4,128)S(1)}, f32[4,128]{1,0:T(4,128)S(1)}, u32[]{:S(2)}, u32[]{:S(2)}) collective-permute-start(f32[4,128]{1,0:T(4,128)S(1)} %broadcast_add_fusion.1), channel_id=1, source_target_pairs={{0,24},{4,28},{1,25},{5,29},{2,26},{6,30},{3,27},{7,31}} | collective-permute-start | bytes 6152 | tf_op jit(solution)/shard_map/ppermute | solution.py:38
  83.6 3.7 %collective-permute-start.13 = (f32[4,128]{1,0:T(4,128)S(1)}, f32[4,128]{1,0:T(4,128)S(1)}, u32[]{:S(2)}, u32[]{:S(2)}) collective-permute-start(f32[4,128]{1,0:T(4,128)S(1)} %broadcast_add_fusion.1), channel_id=1, source_target_pairs={{0,28},{1,29},{2,30},{3,31}} | collective-permute-start | bytes 6152 | tf_op jit(solution)/shard_map/ppermute | solution.py:38
  90.0 1.6 collective-permute-start.5
  91.6 6.5 %collective-permute-start.6 = (bf16[128,128]{1,0:T(8,128)(2,1)S(1)}, bf16[128,128]{1,0:T(8,128)(2,1)S(1)}, u32[]{:S(2)}, u32[]{:S(2)}) collective-permute-start(bf16[128,128]{1,0:T(8,128)(2,1)S(1)} %get-tuple-element.251), channel_id=1, source_target_pairs={{0,28},{1,29},{2,30},{3,31}} | collective-permute-start | bytes 98312 | tf_op jit(solution)/shard_map/ppermute | solution.py:38
  98.3 1.5 collective-permute-done.6
  99.8 5.7 %conditional.1 = (f32[8,128,128]{1,2,0:T(8,128)}, bf16[128,256]{1,0:T(8,128)(2,1)S(1)}) conditional(s32[]{:T(128)} %convert_element_type.39, () %tuple.37, (s32[8,128]{1,0:T(8,128)S(1)}, s32[]{:T(128)}, s32[128]{0:T(128)S(1)}, bf16[8,128,128]{2,1,0:T(8,128)(2,1)S(1)}, bf16[128,256]{1,0:T(8,128)(2,1)}, /*index=5*/f32[4,128]{1,0:T(4,128)S(1)}, ...), branch_computations={%region_6.7_spmd, %region_7.8_spmd} | conditional | flops 340656256 | bytes 14708356 | solution.py:130
  101.0 1.6 fusion.21
  106.6 1.3 collective-permute-start.21
  107.9 1.3 collective-permute-start.20
  109.2 1.3 collective-permute-start.19
  113.1 2.4 %collective-permute-done.21 = f32[128,128]{0,1:T(8,128)S(1)} collective-permute-done((f32[128,128]{0,1:T(8,128)S(1)}, f32[128,128]{0,1:T(8,128)S(1)}, u32[]{:S(2)}, u32[]{:S(2)}) %collective-permute-start.21) | collective-permute-done | bytes 65568 | tf_op jit(solution)/shard_map/ppermute | solution.py:38
  120.0 3.5 %all-to-all-start = ((bf16[4,128,512]{1,2,0:T(8,128)(2,1)}), bf16[4,128,512]{1,2,0:T(8,128)(2,1)S(1)}, u32[]{:S(2)}, u32[]{:S(2)}) async-start(bf16[4,128,512]{1,2,0:T(8,128)(2,1)} %stack.76), calls=%async_computation | async-start | bytes 1048576 | tf_op jit(solution)/shard_map/all_to_all | solution.py:13
  124.2 8.0 %all-to-all-done = bf16[4,128,512]{1,2,0:T(8,128)(2,1)S(1)} async-done(((bf16[4,128,512]{1,2,0:T(8,128)(2,1)}), bf16[4,128,512]{1,2,0:T(8,128)(2,1)S(1)}, u32[]{:S(2)}, u32[]{:S(2)}) %all-to-all-start) | async-done | bytes 524320 | tf_op jit(solution)/shard_map/all_to_all | solution.py:13
  133.4 65.0 %reduce-scatter.2.cloned.1.call-done = f32[256,64]{0,1:T(8,128)} async-done(((f32[2048,64]{0,1:T(8,128)}), f32[256,64]{0,1:T(8,128)}) %reduce-scatter.2.cloned.1.call-update) | async-done | bytes 65552 | tf_op jit(solution)/shard_map/reduce_scatter | solution.py:168
  (99 shorter events, 31.4 us)
Async XLA Ops:
  8.9 81.0 %collective-permute-start = (bf16[128,128]{1,0:T(8,128)(2,1)S(1)}, bf16[128,128]{1,0:T(8,128)(2,1)S(1)}, u32[]{:S(2)}, u32[]{:S(2)}) collective-permute-start(bf16[128,128]{1,0:T(8,128)(2,1)S(1)} %get-tuple-element.251), channel_id=1, source_target_pairs={{0,4},{4,8},{8,12},{12,16},{16,20},{20,24},{24,28},{1,5},{5,9},{9,... | collective-permute-start | bytes 98312 | tf_op jit(solution)/shard_map/ppermute | solution.py:38
  13.8 77.8 %collective-permute-start.1 = (bf16[128,128]{1,0:T(8,128)(2,1)S(1)}, bf16[128,128]{1,0:T(8,128)(2,1)S(1)}, u32[]{:S(2)}, u32[]{:S(2)}) collective-permute-start(bf16[128,128]{1,0:T(8,128)(2,1)S(1)} %get-tuple-element.251), channel_id=1, source_target_pairs={{0,8},{4,12},{8,16},{12,20},{16,24},{20,28},{1,9},{5,13},{9,17},{1... | collective-permute-start | bytes 98312 | tf_op jit(solution)/shard_map/ppermute | solution.py:38
  17.3 80.9 %collective-permute-start.2 = (bf16[128,128]{1,0:T(8,128)(2,1)S(1)}, bf16[128,128]{1,0:T(8,128)(2,1)S(1)}, u32[]{:S(2)}, u32[]{:S(2)}) collective-permute-start(bf16[128,128]{1,0:T(8,128)(2,1)S(1)} %get-tuple-element.251), channel_id=1, source_target_pairs={{0,12},{4,16},{8,20},{12,24},{16,28},{1,13},{5,17},{9,21},{13,25},... | collective-permute-start | bytes 98312 | tf_op jit(solution)/shard_map/ppermute | solution.py:38
  21.8 76.4 %collective-permute-start.3 = (bf16[128,128]{1,0:T(8,128)(2,1)S(1)}, bf16[128,128]{1,0:T(8,128)(2,1)S(1)}, u32[]{:S(2)}, u32[]{:S(2)}) collective-permute-start(bf16[128,128]{1,0:T(8,128)(2,1)S(1)} %get-tuple-element.251), channel_id=1, source_target_pairs={{0,16},{4,20},{8,24},{12,28},{1,17},{5,21},{9,25},{13,29},{2,18},{... | collective-permute-start | bytes 98312 | tf_op jit(solution)/shard_map/ppermute | solution.py:38
  46.1 6.5 %collective-permute-start.7 = (f32[4,128]{1,0:T(4,128)S(1)}, f32[4,128]{1,0:T(4,128)S(1)}, u32[]{:S(2)}, u32[]{:S(2)}) collective-permute-start(f32[4,128]{1,0:T(4,128)S(1)} %broadcast_add_fusion.1), channel_id=1, source_target_pairs={{0,4},{4,8},{8,12},{12,16},{16,20},{20,24},{24,28},{1,5},{5,9},{9,... | collective-permute-start | bytes 6152 | tf_op jit(solution)/shard_map/ppermute | solution.py:38
  52.6 2.8 %collective-permute-start.8 = (f32[4,128]{1,0:T(4,128)S(1)}, f32[4,128]{1,0:T(4,128)S(1)}, u32[]{:S(2)}, u32[]{:S(2)}) collective-permute-start(f32[4,128]{1,0:T(4,128)S(1)} %broadcast_add_fusion.1), channel_id=1, source_target_pairs={{0,8},{4,12},{8,16},{12,20},{16,24},{20,28},{1,9},{5,13},{9,17},{1... | collective-permute-start | bytes 6152 | tf_op jit(solution)/shard_map/ppermute | solution.py:38
  55.4 4.8 %collective-permute-start.9 = (f32[4,128]{1,0:T(4,128)S(1)}, f32[4,128]{1,0:T(4,128)S(1)}, u32[]{:S(2)}, u32[]{:S(2)}) collective-permute-start(f32[4,128]{1,0:T(4,128)S(1)} %broadcast_add_fusion.1), channel_id=1, source_target_pairs={{0,12},{4,16},{8,20},{12,24},{16,28},{1,13},{5,17},{9,21},{13,25},... | collective-permute-start | bytes 6152 | tf_op jit(solution)/shard_map/ppermute | solution.py:38
  60.2 7.3 %collective-permute-start.10 = (f32[4,128]{1,0:T(4,128)S(1)}, f32[4,128]{1,0:T(4,128)S(1)}, u32[]{:S(2)}, u32[]{:S(2)}) collective-permute-start(f32[4,128]{1,0:T(4,128)S(1)} %broadcast_add_fusion.1), channel_id=1, source_target_pairs={{0,16},{4,20},{8,24},{12,28},{1,17},{5,21},{9,25},{13,29},{2,18},{... | collective-permute-start | bytes 6152 | tf_op jit(solution)/shard_map/ppermute | solution.py:38
  67.5 6.2 %collective-permute-start.11 = (f32[4,128]{1,0:T(4,128)S(1)}, f32[4,128]{1,0:T(4,128)S(1)}, u32[]{:S(2)}, u32[]{:S(2)}) collective-permute-start(f32[4,128]{1,0:T(4,128)S(1)} %broadcast_add_fusion.1), channel_id=1, source_target_pairs={{0,20},{4,24},{8,28},{1,21},{5,25},{9,29},{2,22},{6,26},{10,30},{3... | collective-permute-start | bytes 6152 | tf_op jit(solution)/shard_map/ppermute | solution.py:38
  73.7 9.9 %collective-permute-start.12 = (f32[4,128]{1,0:T(4,128)S(1)}, f32[4,128]{1,0:T(4,128)S(1)}, u32[]{:S(2)}, u32[]{:S(2)}) collective-permute-start(f32[4,128]{1,0:T(4,128)S(1)} %broadcast_add_fusion.1), channel_id=1, source_target_pairs={{0,24},{4,28},{1,25},{5,29},{2,26},{6,30},{3,27},{7,31}} | collective-permute-start | bytes 6152 | tf_op jit(solution)/shard_map/ppermute | solution.py:38
  83.6 5.0 %collective-permute-start.13 = (f32[4,128]{1,0:T(4,128)S(1)}, f32[4,128]{1,0:T(4,128)S(1)}, u32[]{:S(2)}, u32[]{:S(2)}) collective-permute-start(f32[4,128]{1,0:T(4,128)S(1)} %broadcast_add_fusion.1), channel_id=1, source_target_pairs={{0,28},{1,29},{2,30},{3,31}} | collective-permute-start | bytes 6152 | tf_op jit(solution)/shard_map/ppermute | solution.py:38
  88.6 9.6 %collective-permute-start.4 = (bf16[128,128]{1,0:T(8,128)(2,1)S(1)}, bf16[128,128]{1,0:T(8,128)(2,1)S(1)}, u32[]{:S(2)}, u32[]{:S(2)}) collective-permute-start(bf16[128,128]{1,0:T(8,128)(2,1)S(1)} %get-tuple-element.251), channel_id=1, source_target_pairs={{0,20},{4,24},{8,28},{1,21},{5,25},{9,29},{2,22},{6,26},{10,30},{3... | collective-permute-start | bytes 98312 | tf_op jit(solution)/shard_map/ppermute | solution.py:38
  90.0 8.3 %collective-permute-start.5 = (bf16[128,128]{1,0:T(8,128)(2,1)S(1)}, bf16[128,128]{1,0:T(8,128)(2,1)S(1)}, u32[]{:S(2)}, u32[]{:S(2)}) collective-permute-start(bf16[128,128]{1,0:T(8,128)(2,1)S(1)} %get-tuple-element.251), channel_id=1, source_target_pairs={{0,24},{4,28},{1,25},{5,29},{2,26},{6,30},{3,27},{7,31}} | collective-permute-start | bytes 98312 | tf_op jit(solution)/shard_map/ppermute | solution.py:38
  91.6 8.1 %collective-permute-start.6 = (bf16[128,128]{1,0:T(8,128)(2,1)S(1)}, bf16[128,128]{1,0:T(8,128)(2,1)S(1)}, u32[]{:S(2)}, u32[]{:S(2)}) collective-permute-start(bf16[128,128]{1,0:T(8,128)(2,1)S(1)} %get-tuple-element.251), channel_id=1, source_target_pairs={{0,28},{1,29},{2,30},{3,31}} | collective-permute-start | bytes 98312 | tf_op jit(solution)/shard_map/ppermute | solution.py:38
  105.5 1.1 collective-permute-start.14
  106.6 8.9 %collective-permute-start.21 = (f32[128,128]{0,1:T(8,128)S(1)}, f32[128,128]{0,1:T(8,128)S(1)}, u32[]{:S(2)}, u32[]{:S(2)}) collective-permute-start(f32[128,128]{0,1:T(8,128)S(1)} %get-tuple-element.255), channel_id=1, source_target_pairs={{28,0},{29,1},{30,2},{31,3}} | collective-permute-start | bytes 196616 | tf_op jit(solution)/shard_map/ppermute | solution.py:38
  107.9 8.8 %collective-permute-start.20 = (f32[128,128]{0,1:T(8,128)S(1)}, f32[128,128]{0,1:T(8,128)S(1)}, u32[]{:S(2)}, u32[]{:S(2)}) collective-permute-start(f32[128,128]{0,1:T(8,128)S(1)} %get-tuple-element.256), channel_id=1, source_target_pairs={{24,0},{28,4},{25,1},{29,5},{26,2},{30,6},{27,3},{31,7}} | collective-permute-start | bytes 196616 | tf_op jit(solution)/shard_map/ppermute | solution.py:38
  109.2 14.3 %collective-permute-start.19 = (f32[128,128]{0,1:T(8,128)S(1)}, f32[128,128]{0,1:T(8,128)S(1)}, u32[]{:S(2)}, u32[]{:S(2)}) collective-permute-start(f32[128,128]{0,1:T(8,128)S(1)} %get-tuple-element.257), channel_id=1, source_target_pairs={{20,0},{24,4},{28,8},{21,1},{25,5},{29,9},{22,2},{26,6},{30,10},{2... | collective-permute-start | bytes 196616 | tf_op jit(solution)/shard_map/ppermute | solution.py:38
  110.5 13.0 %collective-permute-start.18 = (f32[128,128]{0,1:T(8,128)S(1)}, f32[128,128]{0,1:T(8,128)S(1)}, u32[]{:S(2)}, u32[]{:S(2)}) collective-permute-start(f32[128,128]{0,1:T(8,128)S(1)} %get-tuple-element.258), channel_id=1, source_target_pairs={{16,0},{20,4},{24,8},{28,12},{17,1},{21,5},{25,9},{29,13},{18,2},{... | collective-permute-start | bytes 196616 | tf_op jit(solution)/shard_map/ppermute | solution.py:38
  111.8 11.7 %collective-permute-start.17 = (f32[128,128]{0,1:T(8,128)S(1)}, f32[128,128]{0,1:T(8,128)S(1)}, u32[]{:S(2)}, u32[]{:S(2)}) collective-permute-start(f32[128,128]{0,1:T(8,128)S(1)} %get-tuple-element.259), channel_id=1, source_target_pairs={{12,0},{16,4},{20,8},{24,12},{28,16},{13,1},{17,5},{21,9},{25,13},... | collective-permute-start | bytes 196616 | tf_op jit(solution)/shard_map/ppermute | solution.py:38
  115.5 8.1 %collective-permute-start.16 = (f32[128,128]{0,1:T(8,128)S(1)}, f32[128,128]{0,1:T(8,128)S(1)}, u32[]{:S(2)}, u32[]{:S(2)}) collective-permute-start(f32[128,128]{0,1:T(8,128)S(1)} %get-tuple-element.260), channel_id=1, source_target_pairs={{8,0},{12,4},{16,8},{20,12},{24,16},{28,20},{9,1},{13,5},{17,9},{2... | collective-permute-start | bytes 196616 | tf_op jit(solution)/shard_map/ppermute | solution.py:38
  116.8 6.8 %collective-permute-start.15 = (f32[128,128]{0,1:T(8,128)S(1)}, f32[128,128]{0,1:T(8,128)S(1)}, u32[]{:S(2)}, u32[]{:S(2)}) collective-permute-start(f32[128,128]{0,1:T(8,128)S(1)} %get-tuple-element.254), channel_id=1, source_target_pairs={{4,0},{8,4},{12,8},{16,12},{20,16},{24,20},{28,24},{5,1},{9,5},{13... | collective-permute-start | bytes 196616 | tf_op jit(solution)/shard_map/ppermute | solution.py:38
  120.0 12.3 %all-to-all-start = ((bf16[4,128,512]{1,2,0:T(8,128)(2,1)}), bf16[4,128,512]{1,2,0:T(8,128)(2,1)S(1)}, u32[]{:S(2)}, u32[]{:S(2)}) async-start(bf16[4,128,512]{1,2,0:T(8,128)(2,1)} %stack.76), calls=%async_computation | async-start | bytes 1048576 | tf_op jit(solution)/shard_map/all_to_all | solution.py:13
  123.5 74.9 %reduce-scatter.2.cloned.1.call-start = ((), (), s32[]{:S(2)}) async-start(), calls=%async_computation.2 | async-start | bytes 589824 | tf_op jit(solution)/shard_map/reduce_scatter | solution.py:168
  (6 other events, 80.6 us)
Sparse Core Ops, SparseCore 0:
  133.5 64.8 reduce-scatter.1
